TPU v7x, 32 devices: a whole 2x2x4 slice. The times are simulated.
32 devices in a mesh: sp: 8 (over z, x), tp: 4 (over y, core).
Axes of the slice: x: 2, y: 2, z: 4, core: 2. Of those that a mesh axis runs over, the one named last changes fastest.
Arguments:
- residual: bfloat16 [2048, 2048], P('sp', 'tp'), may hold values from -6 to 6
- queries: bfloat16 [2048, 1024], P('sp', 'tp'), may hold values from -5.5 to 5.5
- keys: bfloat16 [2048, 128], P('sp'), may hold values from -5.5 to 5.5
- values: bfloat16 [2048, 128], P('sp'), may hold values from -6 to 6
- documents: int32 [2048], P('sp'), may hold values from 0 to 3, never falling along the last dimension, each value on 1 to 1024 neighbouring positions
- sinks: float32 [16], P('tp'), may hold values from 1 to 6
- head_gain: float32 [1024], replicated, may hold values from 0.1 to 1.9
- out_weight: bfloat16 [1024, 2048], P(None, 'tp'), may hold values from -0.1875 to 0.1875
- norm_gain: float32 [2048], P('tp'), may hold values from 0.1 to 1.9
- norm_shift: float32 [2048], P('tp'), may hold values from -3 to 3
- routes: int32 [2048, 2], P('sp'), may hold values from 0 to 7, all different within a row; in each aligned block of 256 rows (0 to 255, 256 to 511, ...) at most 96 rows name the same one
- route_logits: float32 [2048, 2], P('sp'), may hold values from -150 to 150
- gate_weight: bfloat16 [8, 2048, 6144], P('sp', None, 'tp'), may hold values from -0.125 to 0.125
- up_weight: bfloat16 [8, 2048, 6144], P('sp', None, 'tp'), may hold values from -0.125 to 0.125
- down_weight: bfloat16 [8, 6144, 2048], P('sp', 'tp'), may hold values from -0.15625 to 0.15625
- final_gain: float32 [2048], P('tp'), may hold values from 0.1 to 1.9
- final_shift: float32 [2048], P('tp'), may hold values from -3 to 3
Outputs:
- layer_out: bfloat16 [2048, 2048], P('sp', 'tp')
Inputs may be any that keep to these rules, and one draw needn't show every extreme that they name: `documents`: document numbers never fall along the sequence; each document has at least one position and at most 1024, and some document has exactly 1024. `routes`: each row names 2 different experts. In each aligned block of 256 rows (the rows of one index of sp) no expert is named by more than 96 rows, a bound that some block reaches.
All inputs are finite; a program needn't handle non-finite values.
Results may differ from a plain program's by a relative error of at most 0.014.
Values may be sent and summed in bfloat16 or wider, within the bound.
A program may use at most 128 MiB of HBM per device.

v0:
```python
import jax
import jax.numpy as jnp
from jax import lax
from jax.sharding import PartitionSpec as P

D = 2048
QUERY_HEADS = 16
KEY_VALUE_HEADS = 2
HEAD_SIZE = 64
WINDOW_SIZE = 128
TOP = 2


DEEP_ALPHA = 8.0**0.25
NORM_EPS = 1e-05


def shifted(block, axis, distance):
    devices = range(lax.axis_size(axis))
    route = [(i - distance, i) for i in devices if i - distance in devices]
    return lax.ppermute(block, axis, route)


def split_norm(total, gain, shift):
    totals = lax.psum((jnp.sum(total, axis=1), jnp.sum(total * total, axis=1)), "tp")
    center = totals[0] / D
    spread = totals[1] / D - center * center
    return (total - center[:, None]) * lax.rsqrt(spread + NORM_EPS)[:, None] * gain + shift


def expert_rows(arrived, gate_weight, up_weight, down_weight):
    sources, count, width = arrived.shape
    flat_rows = arrived.reshape(sources * count, width)
    gate = jnp.dot(flat_rows, gate_weight[0], preferred_element_type=jnp.float32)
    up_val = jnp.dot(flat_rows, up_weight[0], preferred_element_type=jnp.float32)
    middle = (jax.nn.silu(gate) * up_val).astype(jnp.bfloat16)
    share_out = jnp.dot(middle, down_weight[0], preferred_element_type=jnp.float32).astype(
        jnp.bfloat16
    )
    share_wide = lax.optimization_barrier(share_out).astype(jnp.float32)
    summed = lax.psum_scatter(
        share_wide.reshape(sources, count, width).astype(jnp.bfloat16),
        "tp",
        scatter_dimension=2,
        tiled=True,
    )
    return lax.all_to_all(summed, "sp", split_axis=0, concat_axis=0, tiled=True)


def pack_rows(source_rows, table, expert_count, capacity):
    padded = jnp.concatenate(
        [source_rows, jnp.zeros((1, source_rows.shape[1]), source_rows.dtype)], axis=0
    )
    return padded[table].reshape(expert_count, capacity, source_rows.shape[1])


def local(
    residual,
    queries,
    keys,
    values,
    documents,
    sinks,
    head_gain,
    out_weight,
    norm_gain,
    norm_shift,
    routes,
    route_logits,
    gate_weight,
    up_weight,
    down_weight,
    final_gain,
    final_shift,
):
    tokens = queries.shape[0]
    head_list = sinks.shape[0]
    tails = shifted(
        (
            keys[tokens - WINDOW_SIZE :],
            values[tokens - WINDOW_SIZE :],
            documents[tokens - WINDOW_SIZE :].astype(jnp.bfloat16),
        ),
        "sp",
        1,
    )
    offset = lax.axis_index("sp") * tokens
    shared_key_head = lax.axis_index("tp") * head_list // (QUERY_HEADS // KEY_VALUE_HEADS)
    all_keys = jnp.concatenate([tails[0], keys], axis=0)
    all_values = jnp.concatenate([tails[1], values], axis=0)
    all_docs = jnp.concatenate([tails[2].astype(jnp.int32), documents], axis=0)
    key_head = lax.dynamic_slice_in_dim(all_keys, shared_key_head * HEAD_SIZE, HEAD_SIZE, 1)
    value_head = lax.dynamic_slice_in_dim(all_values, shared_key_head * HEAD_SIZE, HEAD_SIZE, 1)
    query_heads = queries.reshape(tokens, head_list, HEAD_SIZE)
    scores = jnp.einsum(
        "qhd,kd->hqk", query_heads, key_head, preferred_element_type=jnp.float32
    ) * HEAD_SIZE ** (-0.5)
    query_pos = offset + jnp.arange(tokens, dtype=jnp.int32)
    key_pos = offset - WINDOW_SIZE + jnp.arange(tokens + WINDOW_SIZE, dtype=jnp.int32)
    distance = query_pos[:, None] - key_pos[None, :]
    allowed = (
        (distance >= 0)
        & (distance < WINDOW_SIZE)
        & (key_pos[None, :] >= 0)
        & (documents[:, None] == all_docs[None, :])
    )
    scores = jnp.where(allowed[None], scores, -jnp.inf)
    sink_col = sinks[:, None]
    top = jnp.maximum(jnp.max(scores, axis=2), sink_col)
    expd = jnp.exp(scores - top[..., None])
    probs = (expd / (jnp.sum(expd, axis=2) + jnp.exp(sink_col - top))[..., None]).astype(
        jnp.bfloat16
    )
    attended = jnp.einsum("hqk,kd->qhd", probs, value_head, preferred_element_type=jnp.float32)
    attended = attended.astype(jnp.bfloat16).reshape(tokens, head_list * HEAD_SIZE)
    all_heads = lax.all_gather(attended, "tp", axis=1, tiled=True).astype(jnp.float32)
    scaled = (
        all_heads
        * lax.rsqrt(jnp.mean(all_heads * all_heads, axis=1, keepdims=True) + NORM_EPS)
        * head_gain
    ).astype(jnp.bfloat16)
    mix = jnp.dot(scaled, out_weight, preferred_element_type=jnp.float32)
    first = DEEP_ALPHA * residual.astype(jnp.float32) + mix
    hidden = split_norm(first, norm_gain, norm_shift)
    hidden_rows = hidden.astype(jnp.bfloat16)
    expert_count = lax.axis_size("sp")
    capacity = 3 * tokens * TOP // (2 * expert_count)
    flat = routes.reshape(-1)
    onehot = (flat[:, None] == jnp.arange(expert_count, dtype=jnp.int32)[None, :]).astype(jnp.int32)
    rank = jnp.sum(jnp.cumsum(onehot, axis=0) * onehot, axis=1) - 1
    target = flat * capacity + rank
    owner = jnp.arange(tokens * TOP, dtype=jnp.int32) // TOP
    table = jnp.full((expert_count * capacity,), tokens, jnp.int32).at[target].set(owner)
    outgoing = pack_rows(hidden_rows, table, expert_count, capacity)
    joined = lax.all_gather(
        lax.all_to_all(outgoing, "sp", split_axis=0, concat_axis=0, tiled=True),
        "tp",
        axis=2,
        tiled=True,
    )
    returned = expert_rows(joined, gate_weight, up_weight, down_weight)
    picked = (
        returned.reshape(expert_count * capacity, -1)[target]
        .reshape(tokens, TOP, -1)
        .astype(jnp.float32)
    )
    share = jax.nn.softmax(route_logits, axis=-1)
    moe = jnp.sum(share[:, :, None] * picked, axis=1)
    second = DEEP_ALPHA * hidden + moe
    return split_norm(second, final_gain, final_shift).astype(jnp.bfloat16)


def solution(mesh):
    return jax.shard_map(
        local,
        mesh=mesh,
        in_specs=(
            P("sp", "tp"),
            P("sp", "tp"),
            P("sp", None),
            P("sp", None),
            P("sp"),
            P("tp"),
            P(),
            P(None, "tp"),
            P("tp"),
            P("tp"),
            P("sp", None),
            P("sp", None),
            P("sp", None, "tp"),
            P("sp", None, "tp"),
            P("sp", "tp", None),
            P("tp"),
            P("tp"),
        ),
        out_specs=P("sp", "tp"),
        check_vma=False,
    )
```

profile of v0, /device:TPU:0, one launch (start us, length us, event | category | flops | bytes accessed | tf_op | source)
XLA Modules:
  0.0 207.1 jit_solution(3217525131539474553)
XLA Ops:
  7.3 4.9 %collective-permute-start.1 = (bf16[128]{0:T(256)(128)(2,1)S(1)}, bf16[128]{0:T(256)(128)(2,1)S(1)}, u32[]{:S(2)}, u32[]{:S(2)}) collective-permute-start(bf16[128]{0:T(256)(128)(2,1)S(1)} %slice.17), channel_id=1, source_target_pairs={{0,4},{4,8},{8,12},{12,16},{16,20},{20,24},{24,28},{1,5},{5,9},{9,... | collective-permute-start | bytes 776 | tf_op jit(solution)/shard_map/ppermute | solution.py:21
  12.2 0.9 copy.27
  13.2 3.5 %collective-permute-start.2 = (bf16[128,128]{0,1:T(8,128)(2,1)S(1)}, bf16[128,128]{0,1:T(8,128)(2,1)S(1)}, u32[]{:S(2)}, u32[]{:S(2)}) collective-permute-start(bf16[128,128]{0,1:T(8,128)(2,1)S(1)} %slice.26), channel_id=1, source_target_pairs={{0,4},{4,8},{8,12},{12,16},{16,20},{20,24},{24,28},{1,5},{5,9},{9,... | collective-permute-start | bytes 98312 | tf_op jit(solution)/shard_map/ppermute | solution.py:21
  16.6 0.9 copy.25
  17.6 3.4 %collective-permute-start = (bf16[128,128]{0,1:T(8,128)(2,1)S(1)}, bf16[128,128]{0,1:T(8,128)(2,1)S(1)}, u32[]{:S(2)}, u32[]{:S(2)}) collective-permute-start(bf16[128,128]{0,1:T(8,128)(2,1)S(1)} %slice.25), channel_id=1, source_target_pairs={{0,4},{4,8},{8,12},{12,16},{16,20},{20,24},{24,28},{1,5},{5,9},{9,... | collective-permute-start | bytes 98312 | tf_op jit(solution)/shard_map/ppermute | solution.py:21
  22.8 1.1 reduce-window.6
  24.7 2.4 %scatter_custom_fusion = s32[768]{0:T(1024)S(1)} fusion(s32[512]{0:T(512)S(1)} %bitcast.50, s32[512]{0:T(512)S(1)} %add_select_fusion, s32[]{:T(128)} %constant.80.clone.1), kind=kCustom, calls=%fused_computation.62 | custom fusion | bytes 3076 | tf_op jit(solution)/shard_map/scatter | solution.py:133
  27.1 1.0 copy.29
  28.9 0.9 fusion.23
  31.0 7.2 %all_gather.6 = bf16[256,1024]{0,1:T(8,128)(2,1)S(1)} all-gather(bf16[256,256]{0,1:T(8,128)(2,1)S(1)} %bitcast.48), channel_id=1, replica_groups=mesh['sp'=8,'tp'=4] {'tp'}, dimensions={1}, use_global_device_ids=true | all-gather | bytes 655360 | tf_op jit(solution)/shard_map/all_gather | solution.py:116
  38.4 0.9 fusion.45
  39.3 6.4 %all-reduce.2 = (f32[256]{0:T(256)S(1)}, f32[256]{0:T(256)S(1)}) all-reduce(f32[256]{0:T(256)S(1)} %get-tuple-element.8, f32[256]{0:T(256)S(1)} %get-tuple-element.7), channel_id=1, replica_groups=mesh['sp'=8,'tp'=4] {'tp'}, use_global_device_ids=true, to_apply=%region_6.7 | all-reduce | flops 512 | bytes 4096 | tf_op jit(solution)/shard_map/psum | solution.py:25
  46.0 2.7 %gather_fusion = bf16[768,512]{1,0:T(8,128)(2,1)S(1)} fusion(bf16[257,512]{1,0:T(8,128)(2,1)S(1)} %concatenate.15, s32[1024]{0:T(1024)S(1)} %pad_clamp_fusion.1), kind=kCustom, calls=%fused_computation | custom fusion | bytes 1575936 | tf_op jit(solution)/shard_map/gather | solution.py:54
  48.7 23.2 %all_to_all.10 = bf16[8,96,512]{2,1,0:T(8,128)(2,1)} all-to-all(bf16[8,96,512]{2,1,0:T(8,128)(2,1)S(1)} %bitcast.46), channel_id=1, replica_groups=mesh['sp'=8,'tp'=4] {'sp'}, dimensions={0} | all-to-all | bytes 1572864 | tf_op jit(solution)/shard_map/all_to_all | solution.py:136
  71.9 27.0 %all-gather.2.cloned.1.call-done = bf16[8,96,2048]{2,1,0:T(8,128)(2,1)} async-done(((bf16[8,96,512]{2,1,0:T(8,128)(2,1)}), bf16[8,96,2048]{2,1,0:T(8,128)(2,1)}) %all-gather.2.cloned.1.call-update) | async-done | bytes 3145744 | tf_op jit(solution)/shard_map/all_gather | solution.py:135
  98.9 9.5 %fusion.4 = f32[768,1536]{1,0:T(8,128)} fusion(bf16[768,2048]{1,0:T(8,128)(2,1)} %bitcast.53, bf16[1,2048,1536]{2,1,0:T(8,128)(2,1)} %param.29), kind=kOutput, calls=%fused_computation.7 | convolution fusion | flops 4831838208 | bytes 14155776 | tf_op jit(solution)/shard_map/dot_general | solution.py:34
  108.4 17.2 %fusion.8 = bf16[768,2048]{1,0:T(8,128)(2,1)} fusion(bf16[1,1536,2048]{2,1,0:T(8,128)(2,1)} %param.31, f32[768,1536]{1,0:T(8,128)} %fusion.4, bf16[768,2048]{1,0:T(8,128)(2,1)} %bitcast.54, bf16[1,2048,1536]{2,1,0:T(8,128)(2,1)} %param.30), kind=kOutput, calls=%fused_computation.10 | convolution fusion | flops 9672327168 | bytes 23592960 | tf_op jit(solution)/shard_map/dot_general | solution.py:37
  125.6 37.9 %reduce-scatter.2.cloned.1.call-done = bf16[8,96,512]{2,1,0:T(8,128)(2,1)} async-done(((bf16[8,96,2048]{2,1,0:T(8,128)(2,1)}), bf16[8,96,512]{2,1,0:T(8,128)(2,1)}) %reduce-scatter.2.cloned.1.call-update) | async-done | bytes 786448 | tf_op jit(solution)/shard_map/reduce_scatter | solution.py:41
  163.5 5.5 %all-to-all-start.1 = ((bf16[8,96,512]{2,1,0:T(8,128)(2,1)}), bf16[8,96,512]{2,1,0:T(8,128)(2,1)S(1)}, u32[]{:S(2)}, u32[]{:S(2)}) async-start(bf16[8,96,512]{2,1,0:T(8,128)(2,1)} %reduce-scatter.2.cloned.1.call-done), calls=%async_computation.2 | async-start | bytes 1572864 | tf_op jit(solution)/shard_map/all_to_all | solution.py:47
  169.3 19.9 %all-to-all-done.1 = bf16[8,96,512]{2,1,0:T(8,128)(2,1)S(1)} async-done(((bf16[8,96,512]{2,1,0:T(8,128)(2,1)}), bf16[8,96,512]{2,1,0:T(8,128)(2,1)S(1)}, u32[]{:S(2)}, u32[]{:S(2)}) %all-to-all-start.1) | async-done | bytes 786464 | tf_op jit(solution)/shard_map/all_to_all | solution.py:47
  189.1 2.0 gather_fusion.1
  191.8 1.3 multiply_reduce_fusion
  193.4 5.9 %all-reduce.1 = (f32[256]{0:T(256)S(1)}, f32[256]{0:T(256)S(1)}) all-reduce(f32[256]{0:T(256)S(1)} %get-tuple-element.6, f32[256]{0:T(256)S(1)} %get-tuple-element.5), channel_id=1, replica_groups=mesh['sp'=8,'tp'=4] {'tp'}, use_global_device_ids=true, to_apply=%region_18.19 | all-reduce | flops 512 | bytes 4096 | tf_op jit(solution)/shard_map/psum | solution.py:25
  199.4 0.9 add_convert_fusion
  (68 shorter events, 6.8 us)
Async XLA Ops:
  6.5 31.9 %copy-start = (bf16[1024,512]{1,0:T(8,128)(2,1)S(1)}, bf16[1024,512]{1,0:T(8,128)(2,1)}, u32[]{:S(2)}) copy-start(bf16[1024,512]{1,0:T(8,128)(2,1)} %param.24) | copy-start | bytes 3145732
  6.5 23.7 %copy-start.6 = (f32[4]{0:T(128)S(1)}, f32[4]{0:T(128)}, u32[]{:S(2)}) copy-start(f32[4]{0:T(128)} %param.22) | copy-start | bytes 52
  6.5 92.3 %all-gather.2.cloned.1.call-start = ((), (), s32[]{:S(2)}) async-start(), calls=%async_computation.3 | async-start | bytes 3932160 | tf_op jit(solution)/shard_map/all_gather | solution.py:135
  7.3 20.8 %collective-permute-start.1 = (bf16[128]{0:T(256)(128)(2,1)S(1)}, bf16[128]{0:T(256)(128)(2,1)S(1)}, u32[]{:S(2)}, u32[]{:S(2)}) collective-permute-start(bf16[128]{0:T(256)(128)(2,1)S(1)} %slice.17), channel_id=1, source_target_pairs={{0,4},{4,8},{8,12},{12,16},{16,20},{20,24},{24,28},{1,5},{5,9},{9,... | collective-permute-start | bytes 776 | tf_op jit(solution)/shard_map/ppermute | solution.py:21
  13.2 16.6 %collective-permute-start.2 = (bf16[128,128]{0,1:T(8,128)(2,1)S(1)}, bf16[128,128]{0,1:T(8,128)(2,1)S(1)}, u32[]{:S(2)}, u32[]{:S(2)}) collective-permute-start(bf16[128,128]{0,1:T(8,128)(2,1)S(1)} %slice.26), channel_id=1, source_target_pairs={{0,4},{4,8},{8,12},{12,16},{16,20},{20,24},{24,28},{1,5},{5,9},{9,... | collective-permute-start | bytes 98312 | tf_op jit(solution)/shard_map/ppermute | solution.py:21
  17.6 13.0 %collective-permute-start = (bf16[128,128]{0,1:T(8,128)(2,1)S(1)}, bf16[128,128]{0,1:T(8,128)(2,1)S(1)}, u32[]{:S(2)}, u32[]{:S(2)}) collective-permute-start(bf16[128,128]{0,1:T(8,128)(2,1)S(1)} %slice.25), channel_id=1, source_target_pairs={{0,4},{4,8},{8,12},{12,16},{16,20},{20,24},{24,28},{1,5},{5,9},{9,... | collective-permute-start | bytes 98312 | tf_op jit(solution)/shard_map/ppermute | solution.py:21
  30.6 7.8 %copy-start.7 = (bf16[256,512]{1,0:T(8,128)(2,1)S(1)}, bf16[256,512]{1,0:T(8,128)(2,1)}, u32[]{:S(2)}) copy-start(bf16[256,512]{1,0:T(8,128)(2,1)} %param.17) | copy-start | bytes 786436
  30.6 7.8 %copy-start.8 = (f32[1024]{0:T(1024)S(1)}, f32[1024]{0:T(1024)}, u32[]{:S(2)}) copy-start(f32[1024]{0:T(1024)} %param.23) | copy-start | bytes 12292
  31.0 14.8 %copy-start.2 = (f32[512]{0:T(512)S(1)}, f32[512]{0:T(512)}, u32[]{:S(2)}) copy-start(f32[512]{0:T(512)} %param.26) | copy-start | bytes 6148
  31.0 14.8 %copy-start.3 = (f32[512]{0:T(512)S(1)}, f32[512]{0:T(512)}, u32[]{:S(2)}) copy-start(f32[512]{0:T(512)} %param.25) | copy-start | bytes 6148
  71.9 91.7 %reduce-scatter.2.cloned.1.call-start = ((), (), s32[]{:S(2)}) async-start(), calls=%async_computation.4 | async-start | bytes 3932160 | tf_op jit(solution)/shard_map/reduce_scatter | solution.py:41
  125.6 43.4 %copy-start.1 = (f32[256,2]{0,1:T(2,128)S(1)}, f32[256,2]{0,1:T(2,128)}, u32[]{:S(2)}) copy-start(f32[256,2]{0,1:T(2,128)} %param.28) | copy-start | bytes 6148
  163.5 25.6 %all-to-all-start.1 = ((bf16[8,96,512]{2,1,0:T(8,128)(2,1)}), bf16[8,96,512]{2,1,0:T(8,128)(2,1)S(1)}, u32[]{:S(2)}, u32[]{:S(2)}) async-start(bf16[8,96,512]{2,1,0:T(8,128)(2,1)} %reduce-scatter.2.cloned.1.call-done), calls=%async_computation.2 | async-start | bytes 1572864 | tf_op jit(solution)/shard_map/all_to_all | solution.py:47
  191.1 8.3 %copy-start.4 = (f32[512]{0:T(512)S(1)}, f32[512]{0:T(512)}, u32[]{:S(2)}) copy-start(f32[512]{0:T(512)} %param.33) | copy-start | bytes 6148
  191.1 8.3 %copy-start.5 = (f32[512]{0:T(512)S(1)}, f32[512]{0:T(512)}, u32[]{:S(2)}) copy-start(f32[512]{0:T(512)} %param.32) | copy-start | bytes 6148
Sparse Core Ops, SparseCore 0:
  72.0 26.8 all-gather.1
  125.8 37.7 reduce-scatter.1
where the time goes:
time: 208 us; the launch traced here: 207 us
  waiting for transfers between devices  84.7 us (41%)
  blocking collectives  42.7 us (21%)
  matrix products  28.4 us (14%)
  starting transfers between devices  17.3 us (8%)
  between operations  13.8 us (7%)
  local copies, waits for them, and re-layouts  12.4 us (6%)
  other arithmetic  7.71 us (4%)
    reduce_scatter x1, waiting for transfers between devices, expert_rows(): lax.psum_scatter(share_wide.reshape(sources, count, width).astype(jnp.bfl...  37.9 us
    all_gather x1, waiting for transfers between devices, local(): lax.all_gather(lax.all_to_all(outgoing, 'sp', split_axis=0, concat_axis=0...  27 us
    all_to_all x1, blocking collectives, local(): lax.all_to_all(outgoing, 'sp', split_axis=0, concat_axis=0, tiled=True)  23.2 us
    all_to_all x1, waiting for transfers between devices, expert_rows(): return lax.all_to_all(summed, 'sp', split_axis=0, concat_axis=0, tiled=True)  19.9 us
    dot_general x1, matrix products, expert_rows(): jnp.dot(middle, down_weight[0], preferred_element_type=jnp.float32)  17.2 us
    psum x2, blocking collectives, split_norm(): lax.psum((jnp.sum(total, axis=1), jnp.sum(total * total, axis=1)), 'tp')  12.4 us
    ppermute x3, starting transfers between devices, shifted(): return lax.ppermute(block, axis, route)  11.7 us
    dot_general x1, matrix products, expert_rows(): jnp.dot(flat_rows, gate_weight[0], preferred_element_type=jnp.float32)  9.51 us
  transfers between devices with their start and end apart: 6, of which 3 were waited for; matrix products, arithmetic and copies ran while one was open for 6% of the time, Pallas kernels for 0%

commit v1 on v0

--- a/solution.py
+++ b/solution.py
@@ -1,6 +1,10 @@
+import functools
+
 import jax
 import jax.numpy as jnp
 from jax import lax
+from jax.experimental import pallas as pl
+from jax.experimental.pallas import tpu as pltpu
 from jax.sharding import PartitionSpec as P
 
 D = 2048
@@ -28,30 +32,286 @@
     return (total - center[:, None]) * lax.rsqrt(spread + NORM_EPS)[:, None] * gain + shift
 
 
-def expert_rows(arrived, gate_weight, up_weight, down_weight):
-    sources, count, width = arrived.shape
-    flat_rows = arrived.reshape(sources * count, width)
-    gate = jnp.dot(flat_rows, gate_weight[0], preferred_element_type=jnp.float32)
-    up_val = jnp.dot(flat_rows, up_weight[0], preferred_element_type=jnp.float32)
-    middle = (jax.nn.silu(gate) * up_val).astype(jnp.bfloat16)
-    share_out = jnp.dot(middle, down_weight[0], preferred_element_type=jnp.float32).astype(
-        jnp.bfloat16
-    )
-    share_wide = lax.optimization_barrier(share_out).astype(jnp.float32)
-    summed = lax.psum_scatter(
-        share_wide.reshape(sources, count, width).astype(jnp.bfloat16),
-        "tp",
-        scatter_dimension=2,
-        tiled=True,
-    )
-    return lax.all_to_all(summed, "sp", split_axis=0, concat_axis=0, tiled=True)
-
-
-def pack_rows(source_rows, table, expert_count, capacity):
-    padded = jnp.concatenate(
-        [source_rows, jnp.zeros((1, source_rows.shape[1]), source_rows.dtype)], axis=0
-    )
-    return padded[table].reshape(expert_count, capacity, source_rows.shape[1])
+def swapped(index, step):
+    partner, bit = index, 1
+    while bit <= step:
+        if step & bit:
+            partner = partner + bit - 2 * bit * lax.rem(lax.div(index, bit), 2)
+        bit *= 2
+    return partner
+
+
+def remote(source, target, sems, index, device):
+    return pltpu.make_async_remote_copy(
+        src_ref=source,
+        dst_ref=target,
+        send_sem=sems.at[(0,) + index],
+        recv_sem=sems.at[(1,) + index],
+        device_id=device,
+        device_id_type=pl.DeviceIdType.MESH,
+    )
+
+
+def expert_kernel(
+    n_sp,
+    n_tp,
+    group,
+    rows_ref,
+    gate_hbm,
+    up_hbm,
+    down_hbm,
+    back_ref,
+    gate_w,
+    up_w,
+    down_w,
+    gathered,
+    block,
+    middle,
+    parts,
+    from_core,
+    pair_sums,
+    from_y,
+    finished,
+    landed,
+    weight_sems,
+    sp_sems,
+    core_sems,
+    y_sems,
+    core_sum_sems,
+    y_sum_sems,
+    back_sems,
+):
+    f32 = jnp.float32
+    n_y = n_tp // 2
+    cap, width = rows_ref.shape[1:]
+    ff = gate_w.shape[1]
+    sp, tp = lax.axis_index("sp"), lax.axis_index("tp")
+    y, core = lax.div(tp, 2), lax.rem(tp, 2)
+    partner = {"sp": sp, "tp": tp + 1 - 2 * core}
+    y_to = [lax.rem(y + j, n_y) for j in range(n_y)]
+    y_from = [lax.rem(y + n_y - j, n_y) for j in range(n_y)]
+    waiting = []
+
+    weights = [
+        pltpu.make_async_copy(hbm.at[0], vmem, weight_sems.at[i])
+        for i, (hbm, vmem) in enumerate(
+            ((gate_hbm, gate_w), (up_hbm, up_w), (down_hbm, down_w))
+        )
+    ]
+    for copy in weights:
+        copy.start()
+
+    barrier = pltpu.get_barrier_semaphore()
+    for k in range(1, n_sp):
+        pl.semaphore_signal(
+            barrier,
+            inc=1,
+            device_id={"sp": swapped(sp, k), "tp": tp},
+            device_id_type=pl.DeviceIdType.MESH,
+        )
+    for j in range(1, n_tp):
+        pl.semaphore_signal(
+            barrier,
+            inc=1,
+            device_id={"sp": sp, "tp": lax.rem(tp + j, n_tp)},
+            device_id_type=pl.DeviceIdType.MESH,
+        )
+    pl.semaphore_wait(barrier, n_sp + n_tp - 2)
+
+    def launch(copy):
+        copy.start()
+        waiting.append(copy)
+        return copy
+
+    y_copies, core_copies = {}, {}
+
+    def forward(k):
+        if k:
+            sp_copies[k].wait_recv()
+        source = gathered.at[tp, k] if k else rows_ref.at[0]
+        for j in range(1, n_y):
+            device = {"sp": sp, "tp": y_to[j] * 2 + core}
+            y_copies[j, k] = launch(
+                remote(source, gathered.at[tp, k], y_sems, (j - 1, k), device)
+            )
+        core_copies[0, k] = launch(
+            remote(source, gathered.at[tp, k], core_sems, (0, k), partner)
+        )
+
+    sp_copies = {}
+    forward(0)
+    for k in range(1, n_sp):
+        device = {"sp": swapped(sp, k), "tp": tp}
+        sp_copies[k] = launch(
+            remote(rows_ref.at[k], gathered.at[tp, k], sp_sems, (k,), device)
+        )
+    gathered[tp, 0] = rows_ref[0]
+
+    def relay(k):
+        for j in range(1, n_y):
+            y_copies[j, k].wait_recv()
+            here = gathered.at[y_from[j] * 2 + core, k]
+            core_copies[j, k] = launch(remote(here, here, core_sems, (j, k), partner))
+
+    def arrive(k):
+        for j in range(n_y):
+            core_copies[j, k].wait_recv()
+
+    def members(g):
+        return range(g * group, (g + 1) * group)
+
+    def span(g):
+        return pl.ds(g * group, group)
+
+    def compute(g):
+        for t in range(n_tp):
+            block[:, t * width : (t + 1) * width] = gathered[t, span(g)].reshape(
+                group * cap, width
+            )
+        if g == 0:
+            weights[0].wait()
+            weights[1].wait()
+        tile = next(size for size in (512, 384, 256, 128) if ff % size == 0)
+
+        def hidden_tile(n, carry):
+            columns = pl.ds(pl.multiple_of(n * tile, tile), tile)
+            gate = jnp.dot(block[...], gate_w[:, columns], preferred_element_type=f32)
+            up_val = jnp.dot(block[...], up_w[:, columns], preferred_element_type=f32)
+            middle[:, columns] = (gate / (1.0 + jnp.exp(-gate)) * up_val).astype(jnp.bfloat16)
+            return carry
+
+        lax.fori_loop(0, ff // tile, hidden_tile, 0)
+        if g == 0:
+            weights[2].wait()
+
+        def down_tile(n, carry):
+            for c in range(2):
+                columns = pl.ds(pl.multiple_of((2 * n + c) * width, width), width)
+                share_out = jnp.dot(middle[...], down_w[:, columns], preferred_element_type=f32)
+                parts[c, n, span(g)] = share_out.astype(jnp.bfloat16).reshape(group, cap, width)
+            return carry
+
+        lax.fori_loop(0, n_y, down_tile, 0)
+
+    core_sum_copies, y_sum_copies = {}, {}
+
+    def sum_core(g):
+        core_sum_copies[g] = launch(
+            remote(
+                parts.at[1 - core, :, span(g)],
+                from_core.at[:, span(g)],
+                core_sum_sems,
+                (g,),
+                partner,
+            )
+        )
+
+    def sum_y(g):
+        core_sum_copies[g].wait_recv()
+        for j in range(1, n_y):
+            pair_sums[j - 1, span(g)] = (
+                parts[core, y_to[j], span(g)].astype(f32)
+                + from_core[y_to[j], span(g)].astype(f32)
+            ).astype(jnp.bfloat16)
+            y_sum_copies[j, g] = launch(
+                remote(
+                    pair_sums.at[j - 1, span(g)],
+                    from_y.at[j - 1, span(g)],
+                    y_sum_sems,
+                    (j - 1, g),
+                    {"sp": sp, "tp": y_to[j] * 2 + core},
+                )
+            )
+
+    back_copies = []
+
+    def send_back(g):
+        total = parts[core, y, span(g)].astype(f32) + from_core[y, span(g)].astype(f32)
+        for j in range(1, n_y):
+            y_sum_copies[j, g].wait_recv()
+            total = total + from_y[j - 1, span(g)].astype(f32)
+        finished[span(g)] = total.astype(jnp.bfloat16)
+        for k in members(g):
+            if k:
+                device = {"sp": swapped(sp, k), "tp": tp}
+                back_copies.append(
+                    launch(remote(finished.at[k], landed.at[k], back_sems, (k,), device))
+                )
+
+    groups = n_sp // group
+    for k in members(0):
+        if k:
+            forward(k)
+    for g in range(groups + 2):
+        if g + 1 < groups:
+            for k in members(g + 1):
+                forward(k)
+        if g < groups:
+            for k in members(g):
+                relay(k)
+            for k in members(g):
+                arrive(k)
+            compute(g)
+            sum_core(g)
+        if 0 <= g - 1 < groups:
+            sum_y(g - 1)
+        if 0 <= g - 2 < groups:
+            send_back(g - 2)
+    back_ref[0] = finished[0]
+    for k, copy in enumerate(back_copies, 1):
+        copy.wait_recv()
+        back_ref[k] = landed[k]
+    for copy in waiting:
+        copy.wait_send()
+
+
+def expert_rows(outgoing, gate_weight, up_weight, down_weight):
+    n_sp, n_tp = lax.axis_size("sp"), lax.axis_size("tp")
+    _, cap, width = outgoing.shape
+    _, depth, ff = gate_weight.shape
+    group = 1
+    while group * 2 <= n_sp and group * 2 * cap <= 256:
+        group *= 2
+    n_y = n_tp // 2
+    half = jnp.bfloat16
+    dma = pltpu.SemaphoreType.DMA
+    return pl.pallas_call(
+        functools.partial(expert_kernel, n_sp, n_tp, group),
+        out_shape=jax.ShapeDtypeStruct(outgoing.shape, half),
+        in_specs=[pl.BlockSpec(memory_space=pltpu.VMEM)]
+        + [pl.BlockSpec(memory_space=pl.ANY)] * 3,
+        out_specs=pl.BlockSpec(memory_space=pltpu.VMEM),
+        scratch_shapes=[
+            pltpu.VMEM((depth, ff), half),
+            pltpu.VMEM((depth, ff), half),
+            pltpu.VMEM((ff, depth), half),
+            pltpu.VMEM((n_tp, n_sp, cap, width), half),
+            pltpu.VMEM((group * cap, depth), half),
+            pltpu.VMEM((group * cap, ff), half),
+            pltpu.VMEM((2, n_y, n_sp, cap, width), half),
+            pltpu.VMEM((n_y, n_sp, cap, width), half),
+            pltpu.VMEM((n_y - 1, n_sp, cap, width), half),
+            pltpu.VMEM((n_y - 1, n_sp, cap, width), half),
+            pltpu.VMEM((n_sp, cap, width), half),
+            pltpu.VMEM((n_sp, cap, width), half),
+            dma((3,)),
+            dma((2, n_sp)),
+            dma((2, n_y, n_sp)),
+            dma((2, n_y - 1, n_sp)),
+            dma((2, n_sp // group)),
+            dma((2, n_y - 1, n_sp // group)),
+            dma((2, n_sp)),
+        ],
+        compiler_params=pltpu.CompilerParams(
+            collective_id=0, has_side_effects=True, vmem_limit_bytes=60 * 1024 * 1024
+        ),
+        cost_estimate=pl.CostEstimate(
+            flops=6 * n_sp * cap * depth * ff,
+            bytes_accessed=6 * depth * ff,
+            transcendentals=n_sp * cap * ff,
+        ),
+        name="experts",
+    )(outgoing, gate_weight, up_weight, down_weight)
 
 
 def local(
@@ -75,15 +335,23 @@
 ):
     tokens = queries.shape[0]
     head_list = sinks.shape[0]
-    tails = shifted(
-        (
-            keys[tokens - WINDOW_SIZE :],
-            values[tokens - WINDOW_SIZE :],
-            documents[tokens - WINDOW_SIZE :].astype(jnp.bfloat16),
+    tail = shifted(
+        jnp.concatenate(
+            [
+                keys[tokens - WINDOW_SIZE :],
+                values[tokens - WINDOW_SIZE :],
+                jnp.broadcast_to(
+                    documents[tokens - WINDOW_SIZE :, None].astype(jnp.bfloat16),
+                    (WINDOW_SIZE, 128),
+                ),
+            ],
+            axis=1,
         ),
         "sp",
         1,
     )
+    key_width = keys.shape[1]
+    tails = (tail[:, :key_width], tail[:, key_width : 2 * key_width], tail[:, 2 * key_width])
     offset = lax.axis_index("sp") * tokens
     shared_key_head = lax.axis_index("tp") * head_list // (QUERY_HEADS // KEY_VALUE_HEADS)
     all_keys = jnp.concatenate([tails[0], keys], axis=0)
@@ -125,27 +393,29 @@
     hidden_rows = hidden.astype(jnp.bfloat16)
     expert_count = lax.axis_size("sp")
     capacity = 3 * tokens * TOP // (2 * expert_count)
-    flat = routes.reshape(-1)
-    onehot = (flat[:, None] == jnp.arange(expert_count, dtype=jnp.int32)[None, :]).astype(jnp.int32)
-    rank = jnp.sum(jnp.cumsum(onehot, axis=0) * onehot, axis=1) - 1
-    target = flat * capacity + rank
-    owner = jnp.arange(tokens * TOP, dtype=jnp.int32) // TOP
-    table = jnp.full((expert_count * capacity,), tokens, jnp.int32).at[target].set(owner)
-    outgoing = pack_rows(hidden_rows, table, expert_count, capacity)
-    joined = lax.all_gather(
-        lax.all_to_all(outgoing, "sp", split_axis=0, concat_axis=0, tiled=True),
-        "tp",
-        axis=2,
-        tiled=True,
-    )
-    returned = expert_rows(joined, gate_weight, up_weight, down_weight)
-    picked = (
-        returned.reshape(expert_count * capacity, -1)[target]
-        .reshape(tokens, TOP, -1)
-        .astype(jnp.float32)
-    )
+    slots = -(-capacity // 16) * 16
+    chosen = routes[:, :, None] == jnp.arange(expert_count, dtype=jnp.int32)[None, None, :]
+    named = jnp.any(chosen, axis=1).astype(jnp.bfloat16)
+    earlier = jnp.tril(jnp.ones((tokens, tokens), jnp.bfloat16), -1)
+    ahead = jnp.dot(earlier, named, preferred_element_type=jnp.float32)
+    rank = jnp.sum(jnp.where(chosen, ahead[:, None, :], 0.0), axis=2).astype(jnp.int32)
+    target = jnp.bitwise_xor(routes, lax.axis_index("sp")) * slots + rank
+    places = jnp.arange(expert_count * slots, dtype=jnp.int32)[None, :]
+    picks = [(target[:, r : r + 1] == places).astype(jnp.bfloat16) for r in range(TOP)]
+    outgoing = lax.dot_general(
+        sum(picks[1:], picks[0]),
+        hidden_rows,
+        (((0,), (0,)), ((), ())),
+        preferred_element_type=jnp.float32,
+    ).astype(jnp.bfloat16)
+    returned = expert_rows(
+        outgoing.reshape(expert_count, slots, -1), gate_weight, up_weight, down_weight
+    ).reshape(expert_count * slots, -1)
     share = jax.nn.softmax(route_logits, axis=-1)
-    moe = jnp.sum(share[:, :, None] * picked, axis=1)
+    moe = sum(
+        share[:, r : r + 1] * jnp.dot(picks[r], returned, preferred_element_type=jnp.float32)
+        for r in range(TOP)
+    )
     second = DEEP_ALPHA * hidden + moe
     return split_norm(second, final_gain, final_shift).astype(jnp.bfloat16)
 

time: 208 us -> 110 us (0.53)
  the two profiles are of different devices: /device:TPU:0 before, /device:TPU:10 now
where the time goes in v1:
time: 110 us; the launch traced here: 109 us
  Pallas kernels  67 us (61%)
  blocking collectives  20.7 us (19%)
  other arithmetic  7.95 us (7%)
  matrix products  6.74 us (6%)
  starting transfers between devices  3.46 us (3%)
  local copies, waits for them, and re-layouts  3.06 us (3%)
    pallas_call x1, Pallas kernels, expert_rows(): pl.pallas_call(functools.partial(expert_kernel, n_sp, n_tp, group), out_s...  67 us
    psum x2, blocking collectives, split_norm(): lax.psum((jnp.sum(total, axis=1), jnp.sum(total * total, axis=1)), 'tp')  13.5 us
    all_gather x1, blocking collectives, local(): lax.all_gather(attended, 'tp', axis=1, tiled=True).astype(jnp.float32)  7.2 us
    ppermute x1, starting transfers between devices, shifted(): return lax.ppermute(block, axis, route)  3.46 us
    dot_general x2, matrix products, local(): jnp.dot(picks[r], returned, preferred_element_type=jnp.float32)  3.29 us
    unnamed x19, local copies, waits for them, and re-layouts  3.01 us
  transfers between devices with their start and end apart: 1, of which 0 were waited for; matrix products, arithmetic and copies ran while one was open for 5% of the time, Pallas kernels for 0%

profile of v1, /device:TPU:10, one launch (start us, length us, event | category | flops | bytes accessed | tf_op | source)
XLA Modules:
  0.0 109.2 jit_solution(3406426477838628248)
XLA Ops:
  0.0 1.0 copy.34
  1.1 0.9 copy.35
  2.0 0.7 convert.4
  2.7 3.5 %collective-permute-start = (bf16[128,384]{0,1:T(8,128)(2,1)S(1)}, bf16[128,384]{0,1:T(8,128)(2,1)S(1)}, u32[]{:S(2)}, u32[]{:S(2)}) collective-permute-start(bf16[128,384]{0,1:T(8,128)(2,1)S(1)} %pad_maximum_fusion), channel_id=1, source_target_pairs={{0,4},{4,8},{8,12},{12,16},{16,20},{20,24},{24,28},{1,5},{5,9},{9,... | collective-permute-start | bytes 294920 | tf_op jit(solution)/shard_map/ppermute | solution.py:25
  6.3 1.0 copy.38
  7.3 0.7 fusion.39
  8.2 0.7 select_reduce_fusion
  8.9 0.7 convert_add_fusion
  9.6 0.7 reduce_max.19
  10.3 0.7 fusion.41
  11.0 0.7 fusion.40
  11.8 0.7 pad_add_fusion
  12.5 0.9 fusion.21
  13.4 0.4 fusion.54
  14.2 0.4 convolution_convert_fusion.1
  14.6 7.2 %all_gather.3 = bf16[256,1024]{0,1:T(8,128)(2,1)S(1)} all-gather(bf16[256,256]{0,1:T(8,128)(2,1)S(1)} %bitcast.30), channel_id=1, replica_groups=mesh['sp'=8,'tp'=4] {'tp'}, dimensions={1}, use_global_device_ids=true | all-gather | bytes 655360 | tf_op jit(solution)/shard_map/all_gather | solution.py:384
  22.0 0.9 fusion.50
  22.9 6.4 %all-reduce.1 = (f32[256]{0:T(256)S(1)}, f32[256]{0:T(256)S(1)}) all-reduce(f32[256]{0:T(256)S(1)} %get-tuple-element.8, f32[256]{0:T(256)S(1)} %get-tuple-element.7), channel_id=1, replica_groups=mesh['sp'=8,'tp'=4] {'tp'}, use_global_device_ids=true, to_apply=%region_6.7 | all-reduce | flops 512 | bytes 4096 | tf_op jit(solution)/shard_map/psum | solution.py:29
  29.4 1.5 %convolution_convert_fusion = bf16[768,512]{1,0:T(8,128)(2,1)} fusion(s32[256]{0:T(256)S(1)} %bitcast.32, s32[256]{0:T(256)S(1)} %bitcast.34, f32[256,512]{1,0:T(8,128)S(1)} %get-tuple-element.25, f32[512]{0:T(512)S(1)} %copy-done.6, f32[512]{0:T(512)S(1)} %copy-done.7, f32[256]{0:T(256)S(1)} %get-tuple-element.22, f32[256]{0:T(256)S(1)} %get-tuple-element.21), kind=kOutput, calls=%fused_computation.3 | convolution fusion | flops 203948032 | bytes 1318912 | tf_op jit(solution)/shard_map/dot_general | solution.py:405
  30.9 67.0 %experts.1 = bf16[8,96,512]{2,1,0:T(8,128)(2,1)} custom-call(bf16[8,96,512]{2,1,0:T(8,128)(2,1)} %bitcast.40, bf16[1,2048,1536]{2,1,0:T(8,128)(2,1)} %gate_hbm.1, bf16[1,2048,1536]{2,1,0:T(8,128)(2,1)} %up_hbm.1, bf16[1,1536,2048]{2,1,0:T(8,128)(2,1)} %down_hbm.1), custom_call_target="tpu_custom_call" | custom-call | flops 14495514624 | bytes 18874368 | tf_op jit(solution)/shard_map/experts/pallas_call | solution.py:278
  97.9 1.5 %convolution_multiply_fusion.1 = f32[256,512]{1,0:T(8,128)S(1)} fusion(bf16[768,512]{1,0:T(8,128)(2,1)} %bitcast.38, s32[256]{0:T(256)S(1)} %bitcast.35, f32[256]{0:T(256)S(1)} %bitcast.37), kind=kOutput, calls=%fused_computation.11 | convolution fusion | flops 201654272 | bytes 1312768 | tf_op jit(solution)/shard_map/dot_general | solution.py:416
  99.5 1.7 %fusion.49 = (f32[256]{0:T(256)S(1)}, f32[256]{0:T(256)S(1)}, f32[256,512]{1,0:T(8,128)S(1)}) fusion(f32[256,512]{1,0:T(8,128)S(1)} %convolution_multiply_fusion.1, bf16[768,512]{1,0:T(8,128)(2,1)} %bitcast.39, s32[256]{0:T(256)S(1)} %bitcast.33, f32[256]{0:T(256)S(1)} %bitcast.36, f32[512]{0:T(512)S(1)} %copy-done.6, f32[512]{0:T(512)S(1)} %copy-done.7, ...), kind=kOutput, calls=%fused_computation.83 | convolution fusion | flops 202964480 | bytes 2369536 | tf_op jit(solution)/shard_map/dot_general | solution.py:416
  101.2 7.1 %all-reduce = (f32[256]{0:T(256)S(1)}, f32[256]{0:T(256)S(1)}) all-reduce(f32[256]{0:T(256)S(1)} %get-tuple-element.6, f32[256]{0:T(256)S(1)} %get-tuple-element.5), channel_id=1, replica_groups=mesh['sp'=8,'tp'=4] {'tp'}, use_global_device_ids=true, to_apply=%region_14.15 | all-reduce | flops 512 | bytes 4096 | tf_op jit(solution)/shard_map/psum | solution.py:29
  108.4 0.9 add_convert_fusion
  (38 shorter events, 0.9 us)
Async XLA Ops:
  0.0 22.0 %copy-start = (bf16[1024,512]{1,0:T(8,128)(2,1)S(1)}, bf16[1024,512]{1,0:T(8,128)(2,1)}, u32[]{:S(2)}) copy-start(bf16[1024,512]{1,0:T(8,128)(2,1)} %param.24) | copy-start | bytes 3145732
  1.0 12.8 %copy-start.3 = (f32[4]{0:T(128)S(1)}, f32[4]{0:T(128)}, u32[]{:S(2)}) copy-start(f32[4]{0:T(128)} %param.22) | copy-start | bytes 52
  2.7 9.0 %collective-permute-start = (bf16[128,384]{0,1:T(8,128)(2,1)S(1)}, bf16[128,384]{0,1:T(8,128)(2,1)S(1)}, u32[]{:S(2)}, u32[]{:S(2)}) collective-permute-start(bf16[128,384]{0,1:T(8,128)(2,1)S(1)} %pad_maximum_fusion), channel_id=1, source_target_pairs={{0,4},{4,8},{8,12},{12,16},{16,20},{20,24},{24,28},{1,5},{5,9},{9,... | collective-permute-start | bytes 294920 | tf_op jit(solution)/shard_map/ppermute | solution.py:25
  14.2 7.8 %copy-start.4 = (bf16[256,512]{1,0:T(8,128)(2,1)S(1)}, bf16[256,512]{1,0:T(8,128)(2,1)}, u32[]{:S(2)}) copy-start(bf16[256,512]{1,0:T(8,128)(2,1)} %param.17) | copy-start | bytes 786436
  14.2 7.8 %copy-start.5 = (f32[1024]{0:T(1024)S(1)}, f32[1024]{0:T(1024)}, u32[]{:S(2)}) copy-start(f32[1024]{0:T(1024)} %param.23) | copy-start | bytes 12292
  22.0 7.4 %copy-start.6 = (f32[512]{0:T(512)S(1)}, f32[512]{0:T(512)}, u32[]{:S(2)}) copy-start(f32[512]{0:T(512)} %param.26) | copy-start | bytes 6148
  22.0 7.4 %copy-start.7 = (f32[512]{0:T(512)S(1)}, f32[512]{0:T(512)}, u32[]{:S(2)}) copy-start(f32[512]{0:T(512)} %param.25) | copy-start | bytes 6148
  99.5 8.9 %copy-start.1 = (f32[512]{0:T(512)S(1)}, f32[512]{0:T(512)}, u32[]{:S(2)}) copy-start(f32[512]{0:T(512)} %param.33) | copy-start | bytes 6148
  99.5 8.9 %copy-start.2 = (f32[512]{0:T(512)S(1)}, f32[512]{0:T(512)}, u32[]{:S(2)}) copy-start(f32[512]{0:T(512)} %param.32) | copy-start | bytes 6148
